TPU v7x, 32 devices: a whole 2x2x4 slice. The times are simulated.
32 devices in a mesh: fs: 8 (over z, x), tp: 4 (over y, core).
Axes of the slice: x: 2, y: 2, z: 4, core: 2. Of those that a mesh axis runs over, the one named last changes fastest.
Arguments:
- saved_input: bfloat16 [24576, 2048], P('fs'), may hold values from -6 to 6
- proj_cot: bfloat16 [3, 24576, 2048], P(None, 'fs', 'tp'), may hold values from -0.0390625 to 0.0390625
- log_cache: float32 [16, 24576], P(None, 'fs'), as said below
- cache_cot: float32 [16, 24576], P(None, 'fs'), may hold values from -0.0390625 to 0.0390625
- proj_master: float32 [3, 2048, 2048], P(None, 'fs', 'tp'), may hold values from -0.125 to 0.125
- factors: bfloat16 [3, 2048, 256], P(None, 'fs'), may hold values from -0.125 to 0.125
- first_moment: float32 [3, 256, 2048], P(None, None, 'tp'), may hold values from -6 to 6
- second_moment: float32 [3, 256, 2048], P(None, None, 'tp'), may hold values from 0.01 to 10
- gate_master: float32 [16, 2048], replicated, may hold values from -0.125 to 0.125
- gate_first: float32 [16, 2048], replicated, may hold values from -6 to 6
- gate_second: float32 [16, 2048], replicated, may hold values from 0.1 to 3
Outputs:
- proj_step: float32 [3, 2048, 2048], P(None, 'fs', 'tp')
- proj_new: float32 [3, 2048, 2048], P(None, 'fs', 'tp')
- proj_copy: bfloat16 [3, 2048, 2048], P(None, None, 'tp')
- first_new: float32 [3, 256, 2048], P(None, None, 'tp')
- second_new: float32 [3, 256, 2048], P(None, None, 'tp')
- gate_new: float32 [16, 2048], replicated
- gate_copy: bfloat16 [16, 2048], replicated
- gate_first_new: float32 [16, 2048], replicated
- gate_second_new: float32 [16, 2048], replicated
Inputs may be any that keep to these rules, and one draw needn't show every extreme that they name: `log_cache`: each head's values never rise along positions.
All inputs are finite; a program needn't handle non-finite values.
Results may differ from a plain program's by a relative error of at most 0.0004.
Values may be sent and summed in bfloat16 or wider, within the bound.
A program may use at most 128 MiB of HBM per device.

v0:
```python
import jax
import jax.numpy as jnp
from jax import lax
from jax.sharding import PartitionSpec as P

BETA_ONE = 0.8
BETA_TWO = 0.9
LEARN = 0.001


def from_behind(x, axis, by):
    peers = lax.axis_size(axis)
    pairs = [(i, i + by) for i in range(peers) if 0 <= i + by < peers]
    return lax.ppermute(x, axis, pairs)


def prefix(value, axis, join, neutral):
    count, mine = (lax.axis_size(axis), lax.axis_index(axis))
    pieces = lax.all_gather(value, axis)
    pieces = pieces[::-1]
    mine = count - 1 - mine
    so_far = jnp.full_like(value, 0) + jnp.asarray(neutral, value.dtype)

    def hop(position, so_far):
        longer = join(so_far, pieces[position])
        return jnp.where(position < mine, longer, so_far)

    return lax.fori_loop(0, count - 1, hop, so_far)


def add_pair(earlier, later_part):
    return earlier + later_part


def local(
    saved_input,
    proj_cot,
    log_cache,
    cache_cot,
    proj_master,
    factors,
    first_moment,
    second_moment,
    gate_master,
    gate_first,
    gate_second,
):
    heads = log_cache.shape[0]
    edge = from_behind(log_cache[:, -1:], "fs", 1)
    previous = jnp.concatenate([edge, log_cache[:, :-1]], axis=1)
    gate_logarithm = log_cache - previous
    carried = prefix(jnp.sum(cache_cot, axis=1), "fs", add_pair, jnp.zeros((heads,), jnp.float32))
    later = jnp.flip(jnp.cumsum(jnp.flip(cache_cot, 1), axis=1), 1) + carried[:, None]
    gate_cot = (later * -jnp.expm1(gate_logarithm)).astype(jnp.bfloat16)
    gate_part = jnp.dot(gate_cot, saved_input, preferred_element_type=jnp.float32)
    all_factors = lax.all_gather(factors, "fs", axis=1, tiled=True)
    reduced = jnp.einsum(
        "td,rdk->rtk", saved_input, all_factors, preferred_element_type=jnp.float32
    )
    upper_half = lax.optimization_barrier(reduced.astype(jnp.bfloat16))
    lower_half = (reduced - upper_half.astype(jnp.float32)).astype(jnp.bfloat16)
    low_part = jnp.einsum("rtk,rtw->rkw", upper_half, proj_cot, preferred_element_type=jnp.float32)
    low_part = low_part + jnp.einsum(
        "rtk,rtw->rkw", lower_half, proj_cot, preferred_element_type=jnp.float32
    )
    low, gate_grad = lax.psum((low_part, gate_part), "fs")
    first_new = BETA_ONE * first_moment + (1.0 - BETA_ONE) * low
    second_new = BETA_TWO * second_moment + (1.0 - BETA_TWO) * low * low
    direction = first_new / jnp.sqrt(second_new)
    squares = lax.psum(jnp.sum(direction * direction), "tp")
    entries = direction.shape[0] * direction.shape[1] * direction.shape[2] * lax.axis_size("tp")
    scale = lax.rsqrt(squares / entries + 1e-06)
    product = jnp.einsum(
        "rdk,rkw->rdw", factors.astype(jnp.float32), direction, precision=lax.Precision.HIGHEST
    )
    proj_step = scale * product
    proj_new = proj_master - LEARN * proj_step
    proj_copy = lax.all_gather(proj_new.astype(jnp.bfloat16), "fs", axis=1, tiled=True)
    gate_first_new = BETA_ONE * gate_first + (1.0 - BETA_ONE) * gate_grad
    gate_second_new = BETA_TWO * gate_second + (1.0 - BETA_TWO) * gate_grad * gate_grad
    gate_new = gate_master - LEARN * gate_first_new / jnp.sqrt(gate_second_new)
    gate_copy = gate_new.astype(jnp.bfloat16)
    return (
        proj_step,
        proj_new,
        proj_copy,
        first_new,
        second_new,
        gate_new,
        gate_copy,
        gate_first_new,
        gate_second_new,
    )


def solution(mesh):
    placed = (
        P("fs", None),
        P(None, "fs", "tp"),
        P(None, "fs"),
        P(None, "fs"),
        P(None, "fs", "tp"),
        P(None, "fs", None),
        P(None, None, "tp"),
        P(None, None, "tp"),
        P(),
        P(),
        P(),
    )
    return jax.shard_map(
        local,
        mesh=mesh,
        in_specs=placed,
        out_specs=(
            P(None, "fs", "tp"),
            P(None, "fs", "tp"),
            P(None, None, "tp"),
            P(None, None, "tp"),
            P(None, None, "tp"),
            P(),
            P(),
            P(),
            P(),
        ),
        check_vma=False,
    )
```

profile of v0, /device:TPU:0, one launch (start us, length us, event | category | flops | bytes accessed | tf_op | source)
XLA Modules:
  0.0 330.7 jit_solution(11614293912108282255)
XLA Ops:
  7.2 2.0 copy.26
  9.3 0.8 slice.14
  10.1 4.9 %collective-permute-start = (f32[16,1]{1,0:T(8,128)S(1)}, f32[16,1]{1,0:T(8,128)S(1)}, u32[]{:S(2)}, u32[]{:S(2)}) collective-permute-start(f32[16,1]{1,0:T(8,128)S(1)} %slice.14), channel_id=1, source_target_pairs={{0,4},{4,8},{8,12},{12,16},{16,20},{20,24},{24,28},{1,5},{5,9},{9,... | collective-permute-start | bytes 200 | tf_op jit(solution)/shard_map/ppermute | solution.py:14
  15.0 9.3 %rev.10 = f32[16,3072]{1,0:T(8,128)S(1)} reverse(f32[16,3072]{1,0:T(8,128)} %param.16), dimensions={1} | reverse | bytes 393216 | tf_op jit(solution)/shard_map/jit(_flip)/rev | solution.py:53
  24.4 0.1 reduce_sum.19
  24.5 4.6 %reduce-window.6 = f32[16,24,128]{2,1,0:T(8,128)S(1)} reduce-window(f32[16,24,128]{2,1,0:T(8,128)S(1)} %bitcast.36, f32[]{:T(128)} %constant.50.clone.1), window={size=1x1x128 pad=0_0x0_0x127_0}, to_apply=%region_3.4 | reduce-window | flops 6242304 | bytes 393220 | tf_op jit(solution)/shard_map/reduce-window
  29.1 0.2 slice_reduce_fusion
  29.3 0.2 reduce-window.9
  29.5 0.1 broadcast_add_fusion
  29.7 0.6 dynamic-slice
  30.9 0.2 dynamic-update-slice
  31.2 19.9 %all-reduce = f32[128]{0:T(128)S(1)} all-reduce(f32[128]{0:T(128)S(1)} %dynamic-update-slice), channel_id=2, replica_groups=mesh['fs'=8,'tp'=4] {'fs'}, use_global_device_ids=true, to_apply=%add | all-reduce | flops 128 | bytes 1024
  51.1 0.1 reshape.31
  51.2 0.3 while.14
  51.4 1.7 rev.11
  53.2 7.1 %fusion.14 = f32[16,2048]{1,0:T(8,128)} fusion(bf16[3072,2048]{1,0:T(8,128)(2,1)} %param.13, f32[16,3072]{1,0:T(8,128)S(1)} %copy-done.2, f32[16,3071]{1,0:T(8,128)S(1)} %bitcast.34, f32[16,1]{1,0:T(8,128)S(1)} %collective-permute-done, f32[16,3072]{1,0:T(8,128)S(1)} %rev.11, f32[16]{0:T(128)S(1)} %get-tuple-element.88), kind=kOutput, calls=%fused_computation.27 | convolution fusion | flops 201621504 | bytes 13303872 | tf_op jit(solution)/shard_map/dot_general | solution.py:55
  60.3 15.9 %all-gather.4.cloned.1.call-done = bf16[3,2048,256]{1,2,0:T(8,128)(2,1)} async-done(((bf16[3,256,256]{1,2,0:T(8,128)(2,1)}), bf16[3,2048,256]{1,2,0:T(8,128)(2,1)}) %all-gather.4.cloned.1.call-update) | async-done | bytes 3145744 | tf_op jit(solution)/shard_map/all_gather | solution.py:56
  76.1 16.1 %bitcast_convert_fusion = (bf16[3,3072,256]{1,2,0:T(8,128)(2,1)S(1)}, f32[3,256,3072]{2,1,0:T(8,128)}) fusion(bf16[3,2048,256]{1,2,0:T(8,128)(2,1)} %all-gather.4.cloned.1.call-done, bf16[3072,2048]{1,0:T(8,128)(2,1)} %param.13), kind=kOutput, calls=%fused_computation.5 | convolution fusion | flops 9666035712 | bytes 29884416 | tf_op jit(solution)/shard_map/td,rdk->rtk/dot_general | solution.py:57
  92.2 5.3 %fusion.22 = f32[3,256,512]{2,1,0:T(8,128)S(1)} fusion(bf16[3,3072,256]{1,2,0:T(8,128)(2,1)S(1)} %get-tuple-element.141, bf16[3,3072,512]{2,1,0:T(8,128)(2,1)} %param.14), kind=kOutput, calls=%fused_computation.33 | convolution fusion | flops 2415919104 | bytes 15728640 | tf_op jit(solution)/shard_map/rtk,rtw->rkw/dot_general | solution.py:62
  97.6 10.2 %fusion.6 = f32[3,256,512]{2,1,0:T(8,128)} fusion(f32[3,256,512]{2,1,0:T(8,128)S(1)} %fusion.22, bf16[3,3072,512]{2,1,0:T(8,128)(2,1)} %param.14, f32[3,256,3072]{2,1,0:T(8,128)} %get-tuple-element.142, bf16[3,3072,256]{1,2,0:T(8,128)(2,1)S(1)} %get-tuple-element.141), kind=kOutput, calls=%fused_computation.15 | convolution fusion | flops 2423390208 | bytes 26738688 | tf_op jit(solution)/shard_map/rtk,rtw->rkw/dot_general | solution.py:63
  107.8 0.0 all-gather.6.cloned.1.call-start
  107.9 1.3 copy-done.1
  109.2 0.5 copy.28
  109.7 89.2 %all-reduce.4.cloned.1.call-done = (f32[3,256,512]{2,1,0:T(8,128)}, f32[16,2048]{1,0:T(8,128)}) async-done(((f32[3,256,512]{2,1,0:T(8,128)}, f32[16,2048]{1,0:T(8,128)}), (f32[3,256,512]{2,1,0:T(8,128)}, f32[16,2048]{1,0:T(8,128)})) %all-reduce.4.cloned.1.call-update) | async-done | bytes 1703952 | tf_op jit(solution)/shard_map/psum | solution.py:66
  198.9 5.5 %multiply_reduce_fusion = (f32[]{:T(128)}, f32[3,256,512]{2,1,0:T(8,128)}, f32[3,256,512]{2,1,0:T(8,128)}) fusion(f32[3,256,512]{2,1,0:T(8,128)} %get-tuple-element.130, f32[3,256,512]{2,1,0:T(8,128)} %param.20, f32[3,256,512]{2,1,0:T(8,128)} %param.19), kind=kLoop, calls=%fused_computation.12 | loop fusion | flops 3932159 | bytes 7864324 | tf_op jit(solution)/shard_map/reduce_sum | solution.py:70
  204.4 7.6 %psum.22 = f32[]{:T(128)} all-reduce(f32[]{:T(128)} %get-tuple-element.138), channel_id=1, replica_groups=mesh['fs'=8,'tp'=4] {'tp'}, use_global_device_ids=true, to_apply=%region_2.3 | all-reduce | flops 1 | bytes 8 | tf_op jit(solution)/shard_map/psum | solution.py:70
  212.7 4.8 %fusion.20 = (bf16[3,256,512]{1,2,0:T(8,128)(2,1)}, f32[3,256,512]{1,2,0:T(8,128)S(1)}, f32[3,256,512]{1,2,0:T(8,128)}) fusion(f32[3,256,512]{1,2,0:T(8,128)S(1)} %copy.28, bf16[3,256,256]{2,1,0:T(8,128)(2,1)S(1)} %copy-done, f32[3,256,512]{2,1,0:T(8,128)} %get-tuple-element.140, f32[3,256,512]{2,1,0:T(8,128)} %get-tuple-element.139, f32[]{:T(128)S(6)} %rsqrt.5), kind=kOutput, calls=%fused_computation.32 | convolution fusion | flops 1209925632 | bytes 9043972 | tf_op jit(solution)/shard_map/rdk,rkw->rdw/dot_general | solution.py:73
  217.5 3.0 copy.29
  220.6 1.6 copy.30
  222.2 0.8 fusion.18
  223.0 92.6 %all-gather.6.cloned.1.call-done = bf16[3,2048,512]{1,2,0:T(8,128)(2,1)} async-done(((bf16[3,256,512]{1,2,0:T(8,128)(2,1)}), bf16[3,2048,512]{1,2,0:T(8,128)(2,1)}) %all-gather.6.cloned.1.call-update) | async-done | bytes 6291472 | tf_op jit(solution)/shard_map/all_gather | solution.py:78
  315.6 8.6 %copy.31 = bf16[3,2048,512]{2,1,0:T(8,128)(2,1)} copy(bf16[3,2048,512]{1,2,0:T(8,128)(2,1)} %all-gather.6.cloned.1.call-done) | data formatting | bytes 12582912
  (35 shorter events, 0.4 us)
Async XLA Ops:
  7.2 17.2 %copy-start.3 = (f32[16,3072]{1,0:T(8,128)S(1)}, f32[16,3072]{1,0:T(8,128)}, u32[]{:S(2)}) copy-start(f32[16,3072]{1,0:T(8,128)} %param.16) | copy-start | bytes 589828
  7.2 68.9 %all-gather.4.cloned.1.call-start = ((), (), s32[]{:S(2)}) async-start(), calls=%async_computation | async-start | bytes 3538944 | tf_op jit(solution)/shard_map/all_gather | solution.py:56
  9.2 20.5 %copy-start.8 = (u32[32]{0:T(128)S(1)}, u32[32]{0:T(128)}, u32[]{:S(2)}) copy-start(u32[32]{0:T(128)} %constant.60) | copy-start | bytes 388
  9.2 43.9 %copy-start.2 = (f32[16,3072]{1,0:T(8,128)S(1)}, f32[16,3072]{1,0:T(8,128)}, u32[]{:S(2)}) copy-start(f32[16,3072]{1,0:T(8,128)} %param.15) | copy-start | bytes 589828
  9.2 189.7 %all-reduce.4.cloned.1.call-start = ((), (), s32[]{:S(2)}) async-start(), calls=%async_computation.2 | async-start | bytes 3407872 | tf_op jit(solution)/shard_map/psum | solution.py:66
  10.1 43.1 %collective-permute-start = (f32[16,1]{1,0:T(8,128)S(1)}, f32[16,1]{1,0:T(8,128)S(1)}, u32[]{:S(2)}, u32[]{:S(2)}) collective-permute-start(f32[16,1]{1,0:T(8,128)S(1)} %slice.14), channel_id=1, source_target_pairs={{0,4},{4,8},{8,12},{12,16},{16,20},{20,24},{24,28},{1,5},{5,9},{9,... | collective-permute-start | bytes 200 | tf_op jit(solution)/shard_map/ppermute | solution.py:14
  107.8 1.4 copy-start.1
  107.8 207.7 %all-gather.6.cloned.1.call-start = ((), (), s32[]{:S(2)}) async-start(), calls=%async_computation.1 | async-start | bytes 7077888 | tf_op jit(solution)/shard_map/all_gather | solution.py:78
  198.9 13.8 %copy-start = (bf16[3,256,256]{2,1,0:T(8,128)(2,1)S(1)}, bf16[3,256,256]{2,1,0:T(8,128)(2,1)}, u32[]{:S(2)}) copy-start(bf16[3,256,256]{2,1,0:T(8,128)(2,1)} %param.18) | copy-start | bytes 1179652
  220.6 1.6 copy-start.4
  220.6 1.6 copy-start.5
  220.6 1.6 copy-start.6
  220.6 1.6 copy-start.7
Sparse Core Ops, SparseCore 0:
  10.6 65.4 all-gather.3
  107.9 90.9 all-reduce.3
  217.7 97.8 all-gather.5
where the time goes:
time: 332 us; the launch traced here: 331 us
  waiting for transfers between devices  198 us (60%)
  matrix products  43.6 us (13%)
  local copies, waits for them, and re-layouts  30.1 us (9%)
  blocking collectives  27.5 us (8%)
  between operations  15.3 us (5%)
  other arithmetic  11.4 us (3%)
  starting transfers between devices  4.98 us (2%)
    all_gather x1, waiting for transfers between devices, local(): lax.all_gather(proj_new.astype(jnp.bfloat16), 'fs', axis=1, tiled=True)  92.6 us
    psum x1, waiting for transfers between devices, local(): low, gate_grad = lax.psum((low_part, gate_part), 'fs')  89.2 us
    unnamed x1, blocking collectives  19.9 us
    unnamed x28, local copies, waits for them, and re-layouts  17.9 us
    dot_general x1, matrix products, local(): jnp.einsum('td,rdk->rtk', saved_input, all_factors, preferred_element_typ...  16.1 us
    all_gather x1, waiting for transfers between devices, local(): all_factors = lax.all_gather(factors, 'fs', axis=1, tiled=True)  15.9 us
    dot_general x1, matrix products, local(): jnp.einsum('rtk,rtw->rkw', lower_half, proj_cot, preferred_element_type=j...  10.2 us
    rev x1, local copies, waits for them, and re-layouts, local(): jnp.flip(cache_cot, 1)  9.35 us
  transfers between devices with their start and end apart: 4, of which 3 were waited for; matrix products, arithmetic and copies ran while one was open for 9% of the time, Pallas kernels for 0%

commit v1 on v0

v1 whole, which is shorter than its diff:
```python
import functools

import jax
import jax.numpy as jnp
from jax import lax
from jax.experimental import pallas as pl
from jax.experimental.pallas import tpu as pltpu
from jax.sharding import PartitionSpec as P

BETA_ONE = 0.8
BETA_TWO = 0.9
LEARN = 0.001
LANES = 128
HIGH = lax.Precision.HIGHEST
MESH = pl.DeviceIdType.MESH


def ring_order(count):
    wide = max(count // 4, 1)
    tall = count // wide
    if wide == 1 or tall % 2:
        return list(range(count))
    path = [0]
    for row in range(tall):
        across = range(1, wide)
        for column in across if row % 2 == 0 else reversed(across):
            path.append(row * wide + column)
    path += [row * wide for row in range(tall - 1, 0, -1)]
    return path


def pick(table, index):
    found = jnp.int32(table[0])
    for position, value in enumerate(table):
        if position:
            found = jnp.where(index == position, jnp.int32(value), found)
    return found


class Ring:
    def __init__(self, count):
        self.count = count
        self.order = ring_order(count)
        places = [0] * count
        for position, member in enumerate(self.order):
            places[member] = position
        self.me = lax.axis_index("fs")
        self.place = pick(places, self.me)

    def ahead(self, way, by):
        step = by if way == 0 else -by
        return pick(self.order, lax.rem(self.place + step + 2 * self.count, self.count))

    def hops(self, way, half):
        return self.count // 2 if way == half else self.count - 1 - self.count // 2

    def greet(self, partner=None):
        barrier = pltpu.get_barrier_semaphore()
        for way in range(2):
            pl.semaphore_signal(
                barrier, inc=1, device_id={"fs": self.ahead(way, 1)}, device_id_type=MESH
            )
        if partner is not None:
            pl.semaphore_signal(barrier, inc=1, device_id={"tp": partner}, device_id_type=MESH)
        pl.semaphore_wait(barrier, 2 if partner is None else 3)


def remote(source, target, send, receive, device):
    return pltpu.make_async_remote_copy(
        src_ref=source,
        dst_ref=target,
        send_sem=send,
        recv_sem=receive,
        device_id=device,
        device_id_type=MESH,
    )


def spread(ring, pieces, send, receive):
    most = ring.count // 2
    sent = []
    for hop in range(most):
        for number, (half, first, at) in enumerate(pieces):
            for way in range(2):
                if hop >= ring.hops(way, half):
                    continue
                origin = ring.ahead(way, -hop)
                place = at(origin)
                if hop:
                    remote(place, place, send.at[way, number, hop - 1], receive.at[way, number, hop - 1], {"fs": ring.ahead(way, 1)}).wait_recv()
                copy = remote(
                    first if hop == 0 else place,
                    place,
                    send.at[way, number, hop],
                    receive.at[way, number, hop],
                    {"fs": ring.ahead(way, 1)},
                )
                copy.start()
                sent.append(copy)
    for number, (half, first, at) in enumerate(pieces):
        for way in range(2):
            last = ring.hops(way, half)
            place = at(ring.ahead(way, -last))
            remote(place, place, send.at[way, number, last - 1], receive.at[way, number, last - 1], {"fs": ring.ahead(way, 1)}).wait_recv()
    for copy in sent:
        copy.wait_send()


def copy_gather(count, block, out, send, receive):
    ring = Ring(count)
    ring.greet()
    roles, rows, width = block.shape
    part = rows // 2

    def at(role, half, origin):
        return out.at[role, pl.ds(pl.multiple_of(origin * rows + half * part, part), part)]

    pieces = [
        (half, block.at[role, pl.ds(half * part, part)], functools.partial(at, role, half))
        for role in range(roles)
        for half in range(2)
    ]
    for role in range(roles):
        out[role, pl.ds(pl.multiple_of(ring.me * rows, rows), rows)] = block[role]
    spread(ring, pieces, send, receive)


def gather_copies(block, count):
    roles, rows, width = block.shape
    slots = (2, 2 * roles, count // 2)
    return pl.pallas_call(
        functools.partial(copy_gather, count),
        out_shape=jax.ShapeDtypeStruct((roles, rows * count, width), block.dtype),
        in_specs=[pl.BlockSpec(memory_space=pltpu.VMEM)],
        out_specs=pl.BlockSpec(memory_space=pltpu.VMEM),
        scratch_shapes=[pltpu.SemaphoreType.DMA(slots), pltpu.SemaphoreType.DMA(slots)],
        compiler_params=pltpu.CompilerParams(collective_id=2, has_side_effects=True),
    )(block)


def factor_gather(count, block, stats, out, all_stats, send, receive, give, take):
    ring = Ring(count)
    tp = lax.axis_index("tp")
    core = lax.rem(tp, 2)
    partner = tp + 1 - 2 * core
    ring.greet(partner)
    roles, rows, rank = block.shape
    part = rows // 2
    half_rank = rank // 2
    mine = pl.ds(pl.multiple_of(core * half_rank, half_rank), half_rank)

    def at(half, origin):
        return out.at[:, pl.ds(pl.multiple_of(origin * rows + half * part, part), part), mine]

    def stats_at(origin):
        return all_stats.at[origin]

    pieces = [(0, stats, stats_at)] + [
        (half, block.at[:, pl.ds(half * part, part), mine], functools.partial(at, half))
        for half in range(2)
    ]
    all_stats[ring.me] = stats[...]
    out[:, pl.ds(pl.multiple_of(ring.me * rows, rows), rows), :] = block[...]
    most = count // 2
    sent = []

    def arrived(way, number, hop):
        place = pieces[number][2](ring.ahead(way, -hop))
        remote(place, place, send.at[way, number, hop - 1], receive.at[way, number, hop - 1], {"fs": ring.ahead(way, 1)}).wait_recv()
        return place

    def share(way, number, hop, place):
        copy = remote(place, place, give.at[way, number - 1, hop - 1], take.at[way, number - 1, hop - 1], {"tp": partner})
        copy.start()
        sent.append(copy)

    for hop in range(most + 1):
        for number, (half, first, at_origin) in enumerate(pieces):
            for way in range(2):
                hops = ring.hops(way, half)
                if hop > hops:
                    continue
                source = first
                if hop:
                    source = arrived(way, number, hop)
                if hop < hops:
                    copy = remote(
                        source,
                        at_origin(ring.ahead(way, -hop)),
                        send.at[way, number, hop],
                        receive.at[way, number, hop],
                        {"fs": ring.ahead(way, 1)},
                    )
                    copy.start()
                    sent.append(copy)
                if hop and number:
                    share(way, number, hop, source)
    theirs = pl.ds(pl.multiple_of((1 - core) * half_rank, half_rank), half_rank)
    for number, (half, first, at_origin) in enumerate(pieces):
        if not number:
            continue
        for way in range(2):
            for hop in range(1, ring.hops(way, half) + 1):
                origin = ring.ahead(way, -hop)
                place = out.at[:, pl.ds(pl.multiple_of(origin * rows + half * part, part), part), theirs]
                remote(place, place, give.at[way, number - 1, hop - 1], take.at[way, number - 1, hop - 1], {"tp": partner}).wait_recv()
    for copy in sent:
        copy.wait_send()


def gather_factors(block, stats, count):
    roles, rows, rank = block.shape
    slots = (2, 3, count // 2)
    shares = (2, 2, count // 2)
    vmem = pl.BlockSpec(memory_space=pltpu.VMEM)
    return pl.pallas_call(
        functools.partial(factor_gather, count),
        out_shape=(
            jax.ShapeDtypeStruct((roles, rows * count, rank), block.dtype),
            jax.ShapeDtypeStruct((count,) + stats.shape, stats.dtype),
        ),
        in_specs=[vmem, vmem],
        out_specs=(vmem, vmem),
        scratch_shapes=[
            pltpu.SemaphoreType.DMA(slots),
            pltpu.SemaphoreType.DMA(slots),
            pltpu.SemaphoreType.DMA(shares),
            pltpu.SemaphoreType.DMA(shares),
        ],
        compiler_params=pltpu.CompilerParams(collective_id=0, has_side_effects=True),
    )(block, stats)


def sum_over_ring(count, terms, out, came, sums, send, receive, send_more, receive_more):
    ring = Ring(count)
    ring.greet()
    rows = terms.shape[0] // count
    half_width = terms.shape[1] // 2
    most = count // 2

    def own(member, half):
        return terms.at[pl.ds(pl.multiple_of(member * rows, rows), rows), pl.ds(half * half_width, half_width)]

    sent = []

    def wait(way, half, hop):
        slot = came.at[way, half, hop]
        remote(slot, slot, send.at[way, half, hop], receive.at[way, half, hop], {"fs": ring.ahead(way, 1)}).wait_recv()

    for hop in range(most):
        for late in range(2):
            for way in range(2):
                half = way if late == 0 else 1 - way
                hops = ring.hops(way, half)
                if hop >= hops:
                    continue
                term = own(ring.ahead(way, hops - hop), half)
                if hop:
                    wait(way, half, hop - 1)
                    sums[way, half, hop] = came[way, half, hop - 1] + term[...]
                    term = sums.at[way, half, hop]
                copy = remote(term, came.at[way, half, hop], send.at[way, half, hop], receive.at[way, half, hop], {"fs": ring.ahead(way, 1)})
                copy.start()
                sent.append(copy)
    mine = pl.ds(pl.multiple_of(ring.me * rows, rows), rows)
    for half in range(2):
        total = own(ring.me, half)[...]
        for way in range(2):
            last = ring.hops(way, half) - 1
            wait(way, half, last)
            total = total + came[way, half, last]
        out[mine, pl.ds(half * half_width, half_width)] = total

    def at(half, origin):
        return out.at[pl.ds(pl.multiple_of(origin * rows, rows), rows), pl.ds(half * half_width, half_width)]

    pieces = [(half, at(half, ring.me), functools.partial(at, half)) for half in range(2)]
    spread(ring, pieces, send_more, receive_more)
    for copy in sent:
        copy.wait_send()


def ring_sum(terms, count):
    rows, width = terms.shape
    slots = (2, 2, count // 2)
    vmem = pl.BlockSpec(memory_space=pltpu.VMEM)
    held = pltpu.VMEM(slots + (rows // count, width // 2), jnp.float32)
    return pl.pallas_call(
        functools.partial(sum_over_ring, count),
        out_shape=jax.ShapeDtypeStruct(terms.shape, terms.dtype),
        in_specs=[vmem],
        out_specs=vmem,
        scratch_shapes=[held, held] + [pltpu.SemaphoreType.DMA(slots)] * 4,
        compiler_params=pltpu.CompilerParams(collective_id=1, has_side_effects=True),
    )(terms)


def sums_from(values):
    heads, length = values.shape
    blocks = values.reshape(heads, length // LANES, LANES)
    place = jnp.arange(LANES)
    inside = jnp.einsum(
        "hbt,ts->hbs", blocks, (place[:, None] >= place[None, :]).astype(jnp.float32), precision=HIGH
    )
    which = jnp.arange(length // LANES)
    after = jnp.einsum(
        "hb,bc->hc",
        inside[:, :, 0],
        (which[:, None] > which[None, :]).astype(jnp.float32),
        precision=HIGH,
    )
    return (inside + after[:, :, None]).reshape(heads, length)


def local(
    saved_input,
    proj_cot,
    log_cache,
    cache_cot,
    proj_master,
    factors,
    first_moment,
    second_moment,
    gate_master,
    gate_first,
    gate_second,
):
    heads = log_cache.shape[0]
    count = lax.axis_size("fs")
    me = lax.axis_index("fs")
    totals = jnp.sum(cache_cot, axis=1, keepdims=True)
    edges = log_cache[:, -1:]
    stats = jnp.concatenate(
        [totals, edges, jnp.zeros((heads, LANES - 2), jnp.float32)], axis=1
    )
    all_factors, all_stats = gather_factors(factors, stats, count)
    members = jnp.arange(count)[:, None]
    carried = jnp.sum(jnp.where(members > me, all_stats[:, :, 0], 0.0), axis=0)
    edge = jnp.sum(jnp.where(members == me - 1, all_stats[:, :, 1], 0.0), axis=0)
    previous = jnp.concatenate([edge[:, None], log_cache[:, :-1]], axis=1)
    gate_logarithm = log_cache - previous
    later = sums_from(cache_cot) + carried[:, None]
    gate_cot = (later * -jnp.expm1(gate_logarithm)).astype(jnp.bfloat16)
    gate_part = jnp.dot(gate_cot, saved_input, preferred_element_type=jnp.float32)
    reduced = jnp.einsum(
        "td,rdk->rtk", saved_input, all_factors, preferred_element_type=jnp.float32
    )
    upper_half = lax.optimization_barrier(reduced.astype(jnp.bfloat16))
    lower_half = (reduced - upper_half.astype(jnp.float32)).astype(jnp.bfloat16)
    low_part = jnp.einsum("rtk,rtw->rkw", upper_half, proj_cot, preferred_element_type=jnp.float32)
    low_part = low_part + jnp.einsum(
        "rtk,rtw->rkw", lower_half, proj_cot, preferred_element_type=jnp.float32
    )
    roles, rank, width = low_part.shape
    flat_low = low_part.reshape(roles * rank, width)
    flat_gate = gate_part.reshape(-1, width)
    used = flat_low.shape[0] + flat_gate.shape[0]
    spare = -used % (8 * count)
    terms = jnp.concatenate([flat_low, flat_gate, jnp.zeros((spare, width), jnp.float32)])
    total = ring_sum(terms, count)
    low = total[: roles * rank].reshape(low_part.shape)
    gate_grad = total[roles * rank : used].reshape(gate_part.shape)
    first_new = BETA_ONE * first_moment + (1.0 - BETA_ONE) * low
    second_new = BETA_TWO * second_moment + (1.0 - BETA_TWO) * low * low
    direction = first_new / jnp.sqrt(second_new)
    squares = lax.psum(jnp.sum(direction * direction), "tp")
    entries = direction.shape[0] * direction.shape[1] * direction.shape[2] * lax.axis_size("tp")
    scale = lax.rsqrt(squares / entries + 1e-06)
    product = jnp.einsum(
        "rdk,rkw->rdw", factors.astype(jnp.float32), direction, precision=lax.Precision.HIGHEST
    )
    proj_step = scale * product
    proj_new = proj_master - LEARN * proj_step
    proj_copy = gather_copies(proj_new.astype(jnp.bfloat16), count)
    gate_first_new = BETA_ONE * gate_first + (1.0 - BETA_ONE) * gate_grad
    gate_second_new = BETA_TWO * gate_second + (1.0 - BETA_TWO) * gate_grad * gate_grad
    gate_new = gate_master - LEARN * gate_first_new / jnp.sqrt(gate_second_new)
    gate_copy = gate_new.astype(jnp.bfloat16)
    return (
        proj_step,
        proj_new,
        proj_copy,
        first_new,
        second_new,
        gate_new,
        gate_copy,
        gate_first_new,
        gate_second_new,
    )


def solution(mesh):
    placed = (
        P("fs", None),
        P(None, "fs", "tp"),
        P(None, "fs"),
        P(None, "fs"),
        P(None, "fs", "tp"),
        P(None, "fs", None),
        P(None, None, "tp"),
        P(None, None, "tp"),
        P(),
        P(),
        P(),
    )
    return jax.shard_map(
        local,
        mesh=mesh,
        in_specs=placed,
        out_specs=(
            P(None, "fs", "tp"),
            P(None, "fs", "tp"),
            P(None, None, "tp"),
            P(None, None, "tp"),
            P(None, None, "tp"),
            P(),
            P(),
            P(),
            P(),
        ),
        check_vma=False,
    )
```

time: 332 us -> 207 us (0.62)
  waiting for transfers between devices: 198 us -> 0 us
  Pallas kernels: 0 us -> 137 us
  blocking collectives: 27.5 us -> 6.27 us
  local copies, waits for them, and re-layouts: 30.1 us -> 10.2 us
  between operations: 15.3 us -> 1.54 us
  starting transfers between devices: 4.98 us -> 0 us
    pallas_call x0 -> x3, Pallas kernels: none -> 137 us  [the longest x1 67.2 us: gather_copies(): pl.pallas_call(functools.partial(copy_gather, count), out_shape=jax.Shape...]
    all_gather x2 -> x0, waiting for transfers between devices: 108 us -> none  [the longest x1 92.6 us: local(): lax.all_gather(proj_new.astype(jnp.bfloat16), 'fs', axis=1, tiled=True)]
    psum x1 -> x0, waiting for transfers between devices: 89.2 us -> none  [local(): low, gate_grad = lax.psum((low_part, gate_part), 'fs')]
    unnamed x1 -> x0, blocking collectives: 19.9 us -> none
    rev x3 -> x0, local copies, waits for them, and re-layouts: 11.1 us -> none  [the longest x1 9.35 us: local(): jnp.flip(cache_cot, 1)]
    unnamed x28 -> x18, local copies, waits for them, and re-layouts: 17.9 us -> 7.02 us
    another operation x3 -> x0, other arithmetic: 4.88 us -> none
    ppermute x1 -> x0, starting transfers between devices: 4.86 us -> none  [from_behind(): return lax.ppermute(x, axis, pairs)]
  transfers between devices with their start and end apart: 4 -> 0, of which waited for: 3 -> 0; matrix products, arithmetic and copies ran while one was open for 9% -> 0% of each run, Pallas kernels for 0% -> 0%
where the time goes in v1:
time: 207 us; the launch traced here: 206 us
  Pallas kernels  137 us (66%)
  matrix products  43 us (21%)
  local copies, waits for them, and re-layouts  10.2 us (5%)
  other arithmetic  8.31 us (4%)
  blocking collectives  6.27 us (3%)
    pallas_call x1, Pallas kernels, gather_copies(): pl.pallas_call(functools.partial(copy_gather, count), out_shape=jax.Shape...  67.2 us
    pallas_call x1, Pallas kernels, ring_sum(): pl.pallas_call(functools.partial(sum_over_ring, count), out_shape=jax.Sha...  42.3 us
    pallas_call x1, Pallas kernels, gather_factors(): pl.pallas_call(functools.partial(factor_gather, count), out_shape=(jax.Sh...  27.5 us
    dot_general x1, matrix products, local(): jnp.einsum('td,rdk->rtk', saved_input, all_factors, preferred_element_typ...  17.2 us
    dot_general x1, matrix products, local(): jnp.einsum('rtk,rtw->rkw', lower_half, proj_cot, preferred_element_type=j...  9.27 us
    unnamed x18, local copies, waits for them, and re-layouts  7.02 us
    dot_general x1, matrix products, local(): jnp.dot(gate_cot, saved_input, preferred_element_type=jnp.float32)  6.45 us
    psum x1, blocking collectives, local(): squares = lax.psum(jnp.sum(direction * direction), 'tp')  6.27 us

profile of v1, /device:TPU:0, one launch (start us, length us, event | category | flops | bytes accessed | tf_op | source)
XLA Modules:
  0.0 206.3 jit_solution(3483540104577708219)
XLA Ops:
  0.6 0.0 copy-start.1
  0.7 1.1 reduce_sum.36
  1.8 0.1 pad.6.clone
  1.9 0.1 copy.25
  2.0 0.8 slice.21
  2.7 0.7 maximum_maximum_fusion.stats
  3.4 1.0 copy.33
  4.4 0.2 convolution_bitcast_fusion
  4.6 0.1 slice_reduce_fusion
  4.8 0.1 fusion.19
  4.9 0.1 broadcast_add_fusion
  5.0 27.5 %shard_map.178 = (bf16[3,2048,256]{2,1,0:T(8,128)(2,1)}, f32[8,16,128]{2,1,0:T(8,128)}) custom-call(bf16[3,256,256]{2,1,0:T(8,128)(2,1)} %block.1, f32[16,128]{1,0:T(8,128)} %maximum_maximum_fusion.stats), custom_call_target="tpu_custom_call" | custom-call | tf_op jit(solution)/shard_map/pallas_call | solution.py:216
  32.5 1.1 slice_reduce_fusion.2
  33.6 0.1 select_reduce_fusion
  33.7 0.1 copy.27
  33.8 6.5 %fusion.14 = f32[16,2048]{1,0:T(8,128)S(1)} fusion(bf16[3072,2048]{1,0:T(8,128)(2,1)} %param.11, f32[2,8,24,128]{3,2,1,0:T(8,128)S(1)} %bitcast.48, f32[16,3072]{1,0:T(8,128)S(1)} %copy-done.1, f32[16,3071]{1,0:T(8,128)S(1)} %bitcast.47, f32[16,1]{1,0:T(8,128)S(1)} %copy.27, f32[16]{0:T(128)S(1)} %get-tuple-element.28), kind=kOutput, calls=%fused_computation.27 | convolution fusion | flops 201621504 | bytes 13303872 | tf_op jit(solution)/shard_map/dot_general | solution.py:344
  40.3 0.0 slice-start.1
  40.3 17.2 %bitcast_convert_fusion = (bf16[3,3072,256]{1,2,0:T(8,128)(2,1)}, f32[3,256,3072]{2,1,0:T(8,128)}) fusion(bf16[3,2048,256]{2,1,0:T(8,128)(2,1)} %get-tuple-element.11, bf16[3072,2048]{1,0:T(8,128)(2,1)} %param.11), kind=kOutput, calls=%fused_computation.3 | convolution fusion | flops 9666035712 | bytes 29884416 | tf_op jit(solution)/shard_map/td,rdk->rtk/dot_general | solution.py:345
  57.5 4.5 %fusion.25 = f32[3,256,512]{2,1,0:T(8,128)S(1)} fusion(bf16[3,3072,256]{1,2,0:T(8,128)(2,1)} %get-tuple-element.24, bf16[3,3072,512]{2,1,0:T(8,128)(2,1)S(1)} %bitcast.44), kind=kOutput, calls=%fused_computation.44 | convolution fusion | flops 2415919104 | bytes 15728640 | tf_op jit(solution)/shard_map/rtk,rtw->rkw/dot_general | solution.py:350
  62.0 9.3 %fusion.6 = f32[3,256,512]{2,1,0:T(8,128)S(1)} fusion(f32[3,256,512]{2,1,0:T(8,128)S(1)} %fusion.25, bf16[3,3072,512]{2,1,0:T(8,128)(2,1)} %param.12, f32[3,256,3072]{2,1,0:T(8,128)} %get-tuple-element.25, bf16[3,3072,256]{1,2,0:T(8,128)(2,1)} %get-tuple-element.24), kind=kOutput, calls=%fused_computation.14 | convolution fusion | flops 2423390208 | bytes 26738688 | tf_op jit(solution)/shard_map/rtk,rtw->rkw/dot_general | solution.py:351
  71.3 1.3 pad_maximum_fusion.terms
  72.6 42.3 %shard_map.179 = f32[832,512]{1,0:T(8,128)} custom-call(f32[832,512]{1,0:T(8,128)} %pad_maximum_fusion.terms), custom_call_target="tpu_custom_call" | custom-call | tf_op jit(solution)/shard_map/pallas_call | solution.py:288
  115.0 0.8 slice-done.3
  115.9 0.1 reshape.53
  115.9 0.1 copy-done.3
  116.0 0.1 copy-done.4
  116.1 0.8 fusion.21
  116.9 4.2 %multiply_reduce_fusion = (f32[]{:T(128)}, f32[3,256,512]{2,1,0:T(8,128)S(1)}, f32[3,256,512]{2,1,0:T(8,128)}) fusion(f32[3,256,512]{2,1,0:T(8,128)S(1)} %bitcast.45, f32[3,256,512]{2,1,0:T(8,128)} %param.18, f32[3,256,512]{2,1,0:T(8,128)} %param.17), kind=kLoop, calls=%fused_computation.11 | loop fusion | flops 3932159 | bytes 7864324 | tf_op jit(solution)/shard_map/reduce_sum | solution.py:366
  121.0 6.3 %psum.7 = f32[]{:T(128)} all-reduce(f32[]{:T(128)} %get-tuple-element.21), channel_id=1, replica_groups=mesh['fs'=8,'tp'=4] {'tp'}, use_global_device_ids=true, to_apply=%region_4.5 | all-reduce | flops 1 | bytes 8 | tf_op jit(solution)/shard_map/psum | solution.py:366
  128.0 5.2 %fusion.23 = (bf16[3,256,512]{2,1,0:T(8,128)(2,1)}, f32[3,256,512]{2,1,0:T(8,128)}, f32[3,256,512]{2,1,0:T(8,128)}) fusion(f32[3,256,512]{2,1,0:T(8,128)} %param.15, bf16[3,256,256]{2,1,0:T(8,128)(2,1)} %block.1, f32[3,256,512]{2,1,0:T(8,128)} %get-tuple-element.41, f32[3,256,512]{2,1,0:T(8,128)S(1)} %get-tuple-element.42, f32[]{:T(128)S(6)} %rsqrt.5), kind=kOutput, calls=%fused_computation.43 | convolution fusion | flops 1209925632 | bytes 9043972 | tf_op jit(solution)/shard_map/rdk,rkw->rdw/dot_general | solution.py:369
  133.2 67.2 %shard_map.180 = bf16[3,2048,512]{2,1,0:T(8,128)(2,1)} custom-call(bf16[3,256,512]{2,1,0:T(8,128)(2,1)} %get-tuple-element.19.block), custom_call_target="tpu_custom_call" | custom-call | tf_op jit(solution)/shard_map/pallas_call | solution.py:131
  200.4 5.9 %copy.38 = bf16[3,2048,512]{2,1,0:T(8,128)(2,1)} copy(bf16[3,2048,512]{2,1,0:T(8,128)(2,1)} %shard_map.180) | data formatting | bytes 12582912
  (20 shorter events, 0.1 us)
Async XLA Ops:
  0.6 33.1 %copy-start.1 = (f32[16,3072]{1,0:T(8,128)S(1)}, f32[16,3072]{1,0:T(8,128)}, u32[]{:S(2)}) copy-start(f32[16,3072]{1,0:T(8,128)} %param.13) | copy-start | bytes 589828
  33.8 23.7 %slice-start = ((s8[9437184]{0:T(1024)(128)(4,1)}), s8[1048576]{0:T(1024)(128)(4,1)S(1)}, s32[]{:S(2)}) async-start(s8[9437184]{0:T(1024)(128)(4,1)} %bitcast.43), calls=%async_computation | async-start | bytes 2097152
  40.3 17.2 %slice-start.1 = ((s8[9437184]{0:T(1024)(128)(4,1)}), s8[4194304]{0:T(1024)(128)(4,1)S(1)}, s32[]{:S(2)}) async-start(s8[9437184]{0:T(1024)(128)(4,1)} %bitcast.43), calls=%async_computation.1 | async-start | bytes 8388608
  40.3 17.2 %slice-start.2 = ((s8[9437184]{0:T(1024)(128)(4,1)}), s8[4194304]{0:T(1024)(128)(4,1)S(1)}, s32[]{:S(2)}) async-start(s8[9437184]{0:T(1024)(128)(4,1)} %bitcast.43), calls=%async_computation.2 | async-start | bytes 8388608
  115.0 0.9 slice-start.3
  115.0 1.0 copy-start.2
  115.0 1.0 copy-start.3
  115.0 1.1 copy-start.4
  115.0 1.8 slice-start.4
  121.0 12.2 %copy-start = (f32[3,256,512]{2,1,0:T(8,128)}, f32[3,256,512]{2,1,0:T(8,128)S(1)}, u32[]{:S(2)}) copy-start(f32[3,256,512]{2,1,0:T(8,128)S(1)} %get-tuple-element.42) | copy-start | bytes 4718596
